TPU v7x, 32 devices: a whole 2x2x4 slice. The times are simulated.
32 devices in a mesh: sp: 16 (over z, y, x), tp: 2 (over core).
Axes of the slice: x: 2, y: 2, z: 4, core: 2. Of those that a mesh axis runs over, the one named last changes fastest.
Arguments:
- query: bfloat16 [2048, 2048], P('sp', 'tp'), may hold values from -6 to 6
- forget_logit: bfloat16 [2048, 2048], P('sp', 'tp'), may hold values from -7.5 to 7.5
- value: bfloat16 [2048, 2048], P('sp', 'tp'), may hold values from -6 to 6
- out_gate: bfloat16 [2048, 2048], P('sp', 'tp'), may hold values from -6 to 6
- lower_bound: float32 [2048], P('tp'), may hold values from 0.9 to 1, as said below
- head_gain: float32 [2048], P('tp'), may hold values from 0.1 to 1.9
- residual_in: bfloat16 [2048, 2048], P(('sp', 'tp')), may hold values from -6 to 6
- w_out: bfloat16 [2048, 2048], replicated, may hold values from -0.125 to 0.125
- ffn_gain: float32 [2048], replicated, may hold values from 0.1 to 1.9
- routing: int32 [2048, 2], P(('sp', 'tp')), may hold values from 0 to 15, all different within a row; in each aligned block of 64 rows (0 to 63, 64 to 127, ...) at most 16 rows name the same one
- route_weight: float32 [2048, 2], P(('sp', 'tp')), may hold values from 0.25 to 1
- expert_gate: bfloat16 [16, 2048, 1024], P('sp', None, 'tp'), may hold values from -0.125 to 0.125
- expert_up: bfloat16 [16, 2048, 1024], P('sp', None, 'tp'), may hold values from -0.125 to 0.125
- expert_down: bfloat16 [16, 1024, 2048], P('sp', 'tp'), may hold values from -0.1875 to 0.1875
Outputs:
- layer_out: bfloat16 [2048, 2048], P(('sp', 'tp'))
Inputs may be any that keep to these rules, and one draw needn't show every extreme that they name: `routing`: each row names 2 different experts. In each aligned block of 64 rows (the rows of one device) no expert is named by more than 16 rows, a bound that some blocks reach. 1 - lower_bound is at least 1 / 4096.
All inputs are finite; a program needn't handle non-finite values.
Results may differ from a plain program's by a relative error of at most 0.012.
Values may be sent and summed in bfloat16 or wider, within the bound.
A program may use at most 128 MiB of HBM per device.

v0:
```python
import jax
import jax.numpy as jnp
from jax import lax
from jax.sharding import PartitionSpec as P

HEAD_DIM = 128
BLOCK = 16


epsilon = 1e-06
highest = lax.Precision.HIGHEST


def carried_in(part, axis, combine, identity):
    place = lax.axis_index(axis)
    gathered = lax.all_gather(part, axis)
    state = jnp.zeros_like(part) + jnp.asarray(identity, part.dtype)

    def one(hop, state):
        return combine(state, lax.dynamic_index_in_dim(gathered, hop, 0, False))

    return lax.fori_loop(0, place, one, state)


def combine_pair(former, latter):
    return (former[0] * latter[0], latter[0][..., None] * former[1] + latter[1])


def combine_packed(former, latter):
    former_decay = former[..., -1]
    latter_decay = latter[..., -1]
    state_part = latter_decay[..., None] * former[..., :-1] + latter[..., :-1]
    return jnp.concatenate([state_part, (former_decay * latter_decay)[..., None]], axis=-1)


def body(
    query,
    forget_logit,
    value,
    out_gate,
    lower_bound,
    head_gain,
    residual_in,
    w_out,
    ffn_gain,
    routing,
    route_weight,
    expert_gate,
    expert_up,
    expert_down,
):
    length = query.shape[0]
    local_heads = query.shape[1] // HEAD_DIM
    blocks = length // BLOCK
    grid = (blocks, BLOCK, local_heads, HEAD_DIM)
    floor_gate = lower_bound.reshape(local_heads, HEAD_DIM)
    logits = forget_logit.astype(jnp.float32).reshape(grid)
    log_forget = jnp.logaddexp(
        jnp.log(floor_gate), jnp.log1p(-floor_gate) + jax.nn.log_sigmoid(logits)
    )
    key_gate = (1.0 - floor_gate) * jax.nn.sigmoid(-logits)
    queries = query.astype(jnp.float32).reshape(grid)
    values = value.astype(jnp.float32).reshape(grid)
    cumulative = jnp.cumsum(log_forget, axis=1)
    causal = jnp.arange(BLOCK)[:, None] >= jnp.arange(BLOCK)[None, :]
    log_gaps = cumulative[:, :, None] - cumulative[:, None, :]
    decays = jnp.exp(jnp.where(causal[None, :, :, None, None], log_gaps, -jnp.inf))
    scores = jnp.einsum("ntjd,nsjd,ntsjd->njts", queries, key_gate, decays, precision=highest)
    within = jnp.einsum("njts,nsjv->ntjv", scores, values, precision=highest)
    last_log = cumulative[:, -1]
    weighted = key_gate * jnp.exp(last_log[:, None] - cumulative)
    block_states = jnp.einsum("nsjd,nsjv->njdv", weighted, values, precision=highest)
    running_decay, running_state = lax.associative_scan(
        combine_pair, (jnp.exp(last_log), block_states), axis=0
    )
    identity = (
        jnp.ones(floor_gate.shape, jnp.float32),
        jnp.zeros(block_states.shape[1:], jnp.float32),
    )
    packed_total = jnp.concatenate([running_state[-1], running_decay[-1][..., None]], axis=-1)
    packed_identity = jnp.concatenate([identity[1], identity[0][..., None]], axis=-1)
    carried = carried_in(packed_total, "sp", combine_packed, packed_identity)
    carried_state = carried[..., :-1]
    prior_decay = jnp.concatenate([identity[0][None], running_decay[:-1]], axis=0)
    prior_state = jnp.concatenate([identity[1][None], running_state[:-1]], axis=0)
    start_state = prior_state + prior_decay[..., None] * carried_state[None]
    head_out = within + jnp.einsum(
        "ntjd,njdv->ntjv", queries * jnp.exp(cumulative), start_state, precision=highest
    )
    normed_heads = head_out * lax.rsqrt(
        jnp.mean(head_out * head_out, axis=-1, keepdims=True) + epsilon
    )
    gates = jax.nn.silu(out_gate.astype(jnp.float32).reshape(grid))
    mixed = (
        (normed_heads * head_gain.reshape(local_heads, HEAD_DIM) * gates)
        .astype(jnp.bfloat16)
        .reshape(length, -1)
    )
    regrouped = lax.all_to_all(mixed, "tp", split_axis=0, concat_axis=1, tiled=True)
    projected = jnp.dot(regrouped, w_out, preferred_element_type=jnp.float32)
    updated_f = (
        (residual_in.astype(jnp.float32) + projected).astype(jnp.bfloat16).astype(jnp.float32)
    )
    normed = (
        updated_f
        * lax.rsqrt(jnp.mean(updated_f * updated_f, axis=-1, keepdims=True) + epsilon)
        * ffn_gain
    ).astype(jnp.bfloat16)
    half_rows = normed.shape[0]
    top_count = routing.shape[1]
    width = normed.shape[1]
    experts = lax.axis_size("sp")
    capacity = 2 * half_rows * top_count // experts
    flat_routes = routing.reshape(-1)
    one_hot = (flat_routes[:, None] == jnp.arange(experts, dtype=jnp.int32)[None, :]).astype(
        jnp.int32
    )
    slot_rank = jnp.sum(one_hot * (jnp.cumsum(one_hot, axis=0) - 1), axis=1)
    slot_index = flat_routes * capacity + slot_rank
    outbox = (
        jnp.zeros((experts * capacity, width), jnp.bfloat16)
        .at[slot_index]
        .set(jnp.repeat(normed, top_count, axis=0))
    )
    arrived = lax.all_to_all(
        outbox.reshape(experts, capacity, width), "sp", split_axis=0, concat_axis=0, tiled=True
    )
    arrived_rows = arrived.reshape(experts * capacity, width)
    stacked = jnp.stack([expert_gate, expert_up], axis=0)
    piece = lax.all_gather(stacked, "tp", axis=3, tiled=True)
    gate_part = jnp.dot(arrived_rows, piece[0, 0], preferred_element_type=jnp.float32)
    up_part = jnp.dot(arrived_rows, piece[1, 0], preferred_element_type=jnp.float32)
    hidden = (jax.nn.silu(gate_part) * up_part).astype(jnp.bfloat16)
    result = jnp.dot(
        hidden,
        lax.all_gather(expert_down, "tp", axis=1, tiled=True)[0],
        preferred_element_type=jnp.float32,
    )
    expert_out = result.astype(jnp.bfloat16).reshape(experts, capacity, width)
    returned = lax.all_to_all(expert_out, "sp", split_axis=0, concat_axis=0, tiled=True)
    picked = (
        returned.reshape(experts * capacity, width)[slot_index]
        .reshape(half_rows, top_count, width)
        .astype(jnp.float32)
    )
    expert_sum = jnp.sum(picked * route_weight[:, :, None], axis=1)
    return (updated_f + expert_sum).astype(jnp.bfloat16)


def solution(mesh):
    placed = (
        P("sp", "tp"),
        P("sp", "tp"),
        P("sp", "tp"),
        P("sp", "tp"),
        P("tp"),
        P("tp"),
        P(("sp", "tp"), None),
        P(),
        P(),
        P(("sp", "tp"), None),
        P(("sp", "tp"), None),
        P("sp", None, "tp"),
        P("sp", None, "tp"),
        P("sp", "tp", None),
    )
    return jax.shard_map(
        body, mesh=mesh, in_specs=placed, out_specs=P(("sp", "tp"), None), check_vma=False
    )
```

profile of v0, /device:TPU:0, one launch (start us, length us, event | category | flops | bytes accessed | tf_op | source)
XLA Modules:
  0.0 305.3 jit_solution(16403134711104120234)
XLA Ops:
  6.5 0.7 subtract_bitcast_fusion
  7.3 1.1 fusion.28
  8.4 0.1 copy.93
  8.5 0.8 fusion.44
  9.5 1.0 convert_bitcast_fusion
  10.5 0.1 copy.95
  10.6 0.1 copy.94
  10.7 1.2 exponential_multiply_fusion
  11.9 1.9 fusion.39
  13.8 0.6 slice_add_fusion.2
  14.4 0.1 slice_add_fusion.3
  14.5 1.3 copy-done
  15.9 0.1 fusion.70
  16.2 6.4 %pad.43 = f32[4,8,128,128]{2,3,1,0:T(8,128)} pad(f32[2,8,128,128]{2,3,1,0:T(8,128)S(1)} %pad_maximum_fusion.3, f32[]{:T(128)} %constant.19.clone.1), padding=0_1_1x0_0_0x0_0_0x0_0_0 | pad | bytes 3145732 | tf_op jit(solution)/shard_map/pad | solution.py:73
  22.5 6.5 %pad.44 = f32[4,8,128,128]{2,3,1,0:T(8,128)} pad(f32[2,8,128,128]{2,3,1,0:T(8,128)S(1)} %pad_add_fusion, f32[]{:T(128)} %constant.19.clone.1), padding=1_0_1x0_0_0x0_0_0x0_0_0 | pad | bytes 3145732 | tf_op jit(solution)/shard_map/pad | solution.py:73
  29.1 2.5 add.174
  31.6 11.9 %pad.114 = f32[7,8,128,128]{2,3,1,0:T(8,128)} pad(f32[4,8,128,128]{2,3,1,0:T(8,128)S(1)} %add.174, f32[]{:T(128)} %constant.19.clone.1), padding=0_0_1x0_0_0x0_0_0x0_0_0 | pad | bytes 5767172
  43.5 1.1 add_bitcast_fusion
  44.6 0.9 copy.69
  45.6 4.6 %pad_maximum_fusion.1 = bf16[2,1,2048,512]{3,2,1,0:T(8,128)(2,1)} fusion(bf16[1,1,2048,512]{3,2,1,0:T(8,128)(2,1)} %bitcast.144, bf16[1,1,2048,512]{3,2,1,0:T(8,128)(2,1)} %bitcast.145), kind=kLoop, calls=%fused_computation.14 | loop fusion | flops 2097152 | bytes 8388608 | tf_op jit(solution)/shard_map/stack | solution.py:129
  50.2 0.2 all-gather.7.cloned.1.call-start
  50.4 0.5 all-gather.7.cloned.1.call-update
  51.0 12.1 %pad.46 = f32[8,8,128,128]{2,3,1,0:T(8,128)} pad(f32[4,8,128,128]{2,3,1,0:T(8,128)S(1)} %add.174, f32[]{:T(128)} %constant.19.clone.1), padding=1_0_1x0_0_0x0_0_0x0_0_0 | pad | bytes 6291460 | tf_op jit(solution)/shard_map/pad | solution.py:73
  63.1 0.1 copy.79
  63.2 1.0 convert_bitcast_fusion.1
  64.2 0.9 copy.97
  65.1 1.3 exponential_bitcast_fusion
  66.5 0.1 copy.64
  66.7 5.6 %fusion = f32[8,8,16,16]{2,3,1,0:T(8,128)S(1)} fusion(f32[8,8,16,16,128]{4,1,3,2,0:T(8,128)S(1)} %exponential_bitcast_fusion, f32[8,8,128,16]{2,3,1,0:T(8,128)S(1)} %copy.64, f32[8,8,128,16]{2,3,1,0:T(8,128)S(1)} %copy.63), kind=kLoop, calls=%fused_computation.8 | loop fusion | flops 6275072 | bytes 9502720 | tf_op jit(solution)/shard_map/ntjd,nsjd,ntsjd->njts/dot_general | solution.py:68
  72.4 0.6 convolution_bitcast_fusion
  73.0 0.5 fusion.16
  73.5 0.1 pad_maximum_fusion.2
  73.7 12.1 %pad.45 = f32[8,8,128,128]{2,3,1,0:T(8,128)} pad(f32[4,8,128,128]{2,3,1,0:T(8,128)S(1)} %pad_maximum_fusion.2, f32[]{:T(128)} %constant.19.clone.1), padding=0_1_1x0_0_0x0_0_0x0_0_0 | pad | bytes 6291460 | tf_op jit(solution)/shard_map/pad | solution.py:73
  85.9 0.1 copy.78
  86.0 0.1 mul.218
  86.1 0.1 eq.15
  86.4 0.2 reduce_window_sum.23
  86.5 0.2 select_reduce_fusion
  86.7 5.9 %slice_add_fusion.1 = f32[7,8,128,128]{2,3,1,0:T(8,128)} fusion(f32[8,8,128,128]{2,3,1,0:T(8,128)} %pad.46, f32[8,8,128,128]{2,3,1,0:T(8,128)} %pad.45), kind=kLoop, calls=%fused_computation.21 | loop fusion | flops 917504 | bytes 11010048 | tf_op jit(solution)/shard_map/add | solution.py:73
  92.7 91.0 %all-gather.9.cloned.1.call-done = f32[128,128,129]{1,0,2:T(8,128)} async-done(((f32[8,128,129]{1,0,2:T(8,128)}), f32[128,128,129]{1,0,2:T(8,128)}) %all-gather.9.cloned.1.call-update) | async-done | bytes 8454160 | tf_op jit(solution)/shard_map/all_gather | solution.py:16
  183.6 0.2 concatenate.36
  183.8 0.2 while.10
  184.1 0.1 copy.71
  184.3 0.6 copy-done.4
  184.9 8.9 %multiply_reduce_fusion.2 = (f32[8,16,8]{1,2,0:T(8,128)S(1)}, f32[8,16,8,128]{3,1,2,0:T(8,128)S(1)}) fusion(f32[8,16,8,128]{3,1,2,0:T(8,128)S(1)} %convolution_bitcast_fusion, f32[8,16,8,128]{3,2,1,0:T(8,128)S(1)} %copy-done.4, f32[7,8,128,128]{2,3,1,0:T(8,128)} %slice_add_fusion.1, f32[8,128,128]{1,2,0:T(8,128)S(1)} %copy.71, f32[8,8,128]{2,1,0:T(8,128)S(1)} %concatenate.34), kind=kOutput, calls=%fused_computation.78 | convolution fusion | flops 203815936 | bytes 5804032 | tf_op jit(solution)/shard_map/ntjd,njdv->ntjv/dot_general | solution.py:87
  193.8 0.2 multiply_convert_fusion.1
  194.1 0.1 all_to_all.20
  194.3 4.1 %all_to_all.29 = bf16[2,64,1024]{2,1,0:T(8,128)(2,1)S(1)} all-to-all(bf16[2,64,1024]{2,1,0:T(8,128)(2,1)S(1)} %all_to_all.20), channel_id=1, replica_groups=mesh['sp'=16,'tp'=2] {'tp'}, dimensions={0} | all-to-all | bytes 524288 | tf_op jit(solution)/shard_map/all_to_all | solution.py:99
  198.4 5.1 %multiply_reduce_fusion.1 = (f32[64]{0:T(128)S(1)}, f32[64,2048]{1,0:T(8,128)S(1)}) fusion(bf16[64,2048]{1,0:T(8,128)(2,1)S(1)} %bitcast.146, bf16[2048,2048]{1,0:T(8,128)(2,1)} %param.23, bf16[64,2048]{1,0:T(8,128)(2,1)S(1)} %copy-done.7), kind=kOutput, calls=%fused_computation.74 | convolution fusion | flops 537657280 | bytes 9437440 | tf_op jit(solution)/shard_map/dot_general | solution.py:100
  203.6 0.1 multiply_convert_fusion
  203.7 0.3 broadcast_in_dim.22
  204.0 0.2 reshape.172
  204.2 2.5 scatter_custom_fusion
  206.7 23.6 %all-to-all-start.1 = ((bf16[16,16,2048]{2,1,0:T(8,128)(2,1)}), bf16[16,16,2048]{2,1,0:T(8,128)(2,1)S(1)}, u32[]{:S(2)}, u32[]{:S(2)}) async-start(bf16[16,16,2048]{2,1,0:T(8,128)(2,1)} %bitcast.23), calls=%async_computation.1 | async-start | bytes 2097152 | tf_op jit(solution)/shard_map/all_to_all | solution.py:125
  230.3 24.6 %all-to-all-done.1 = bf16[16,16,2048]{2,1,0:T(8,128)(2,1)S(1)} async-done(((bf16[16,16,2048]{2,1,0:T(8,128)(2,1)}), bf16[16,16,2048]{2,1,0:T(8,128)(2,1)S(1)}, u32[]{:S(2)}, u32[]{:S(2)}) %all-to-all-start.1) | async-done | bytes 1048608 | tf_op jit(solution)/shard_map/all_to_all | solution.py:125
  254.9 3.4 %fusion.2 = f32[256,1024]{1,0:T(8,128)S(1)} fusion(bf16[256,2048]{1,0:T(8,128)(2,1)S(1)} %bitcast.147, bf16[2,1,2048,1024]{3,2,1,0:T(8,128)(2,1)} %all-gather.5.cloned.1.call-done), kind=kOutput, calls=%fused_computation.13 | convolution fusion | flops 1073741824 | bytes 6291456 | tf_op jit(solution)/shard_map/dot_general | solution.py:131
  258.4 7.0 %fusion.9 = bf16[256,2048]{1,0:T(8,128)(2,1)} fusion(bf16[1,1024,2048]{2,1,0:T(8,128)(2,1)} %all-gather.7.cloned.1.call-done, bf16[256,2048]{1,0:T(8,128)(2,1)S(1)} %bitcast.148, bf16[2,1,2048,1024]{3,2,1,0:T(8,128)(2,1)} %all-gather.5.cloned.1.call-done, f32[256,1024]{1,0:T(8,128)S(1)} %fusion.2), kind=kOutput, calls=%fused_computation.22 | convolution fusion | flops 2149580800 | bytes 11534336 | tf_op jit(solution)/shard_map/dot_general | solution.py:134
  265.4 6.2 %all-to-all-start.2 = ((bf16[16,16,2048]{2,1,0:T(8,128)(2,1)}), bf16[16,16,2048]{2,1,0:T(8,128)(2,1)S(1)}, u32[]{:S(2)}, u32[]{:S(2)}) async-start(bf16[16,16,2048]{2,1,0:T(8,128)(2,1)} %bitcast.30), calls=%async_computation.2 | async-start | bytes 2097152 | tf_op jit(solution)/shard_map/all_to_all | solution.py:140
  271.6 0.1 copy.80
  271.7 23.2 %all-to-all-done.2 = bf16[16,16,2048]{2,1,0:T(8,128)(2,1)S(1)} async-done(((bf16[16,16,2048]{2,1,0:T(8,128)(2,1)}), bf16[16,16,2048]{2,1,0:T(8,128)(2,1)S(1)}, u32[]{:S(2)}, u32[]{:S(2)}) %all-to-all-start.2) | async-done | bytes 1048608 | tf_op jit(solution)/shard_map/all_to_all | solution.py:140
  294.9 0.9 gather_fusion
  295.8 0.7 reshape.156
  296.5 1.5 multiply_reduce_fusion
  298.0 0.8 add_convert_fusion
  (74 shorter events, 1.1 us)
Async XLA Ops:
  6.5 4.1 %copy-start.8 = (bf16[128,1024]{1,0:T(8,128)(2,1)S(1)}, bf16[128,1024]{1,0:T(8,128)(2,1)}, u32[]{:S(2)}) copy-start(bf16[128,1024]{1,0:T(8,128)(2,1)} %param.18) | copy-start | bytes 786436
  6.5 177.1 %all-gather.9.cloned.1.call-start = ((), (), s32[]{:S(2)}) async-start(), calls=%async_computation.5 | async-start | bytes 8982528 | tf_op jit(solution)/shard_map/all_gather | solution.py:16
  9.4 53.7 %copy-start.9 = (f32[8,8,128]{2,1,0:T(8,128)}, f32[8,8,128]{2,1,0:T(8,128)S(1)}, u32[]{:S(2)}) copy-start(f32[8,8,128]{2,1,0:T(8,128)S(1)} %fusion.69) | copy-start | bytes 98308
  13.8 2.0 copy-start
  45.5 184.8 %all-gather.5.cloned.1.call-start = ((), (), s32[]{:S(2)}) async-start(), calls=%async_computation.3 | async-start | bytes 12582912 | tf_op jit(solution)/shard_map/all_gather | solution.py:130
  50.2 208.2 %all-gather.7.cloned.1.call-start = ((), (), s32[]{:S(2)}) async-start(), calls=%async_computation.4 | async-start | bytes 6291456 | tf_op jit(solution)/shard_map/all_gather | solution.py:136
  50.9 12.2 %copy-start.12 = (s32[64,2]{0,1:T(2,128)S(1)}, s32[64,2]{0,1:T(2,128)}, u32[]{:S(2)}) copy-start(s32[64,2]{0,1:T(2,128)} %param.25) | copy-start | bytes 1540
  65.1 1.5 copy-start.5
  66.7 6.3 %copy-start.1 = (f32[8,8,128,128]{2,3,1,0:T(8,128)S(1)}, f32[8,8,128,128]{2,3,1,0:T(8,128)}, u32[]{:S(2)}) copy-start(f32[8,8,128,128]{2,3,1,0:T(8,128)} %copy-done) | copy-start | bytes 12582916
  66.7 6.3 %copy-start.2 = (f32[4,8,128,128]{2,3,1,0:T(8,128)S(1)}, f32[4,8,128,128]{2,3,1,0:T(8,128)}, u32[]{:S(2)}) copy-start(f32[4,8,128,128]{2,3,1,0:T(8,128)} %pad.43) | copy-start | bytes 6291460
  66.7 6.3 %copy-start.3 = (f32[4,8,128,128]{2,3,1,0:T(8,128)S(1)}, f32[4,8,128,128]{2,3,1,0:T(8,128)}, u32[]{:S(2)}) copy-start(f32[4,8,128,128]{2,3,1,0:T(8,128)} %pad.44) | copy-start | bytes 6291460
  72.4 1.2 slice-start
  73.7 12.1 %slice-start.1 = ((f32[8,8,128]{2,1,0:T(8,128)}), f32[1,8,128]{2,1,0:T(8,128)S(1)}, s32[]{:S(2)}) async-start(f32[8,8,128]{2,1,0:T(8,128)} %copy-done.9), calls=%async_computation.7 | async-start | bytes 8192 | tf_op jit(solution)/shard_map/slice | solution.py:73
  183.8 1.0 copy-start.4
  184.1 9.7 %copy-start.6 = (f32[16,8,8,128]{3,2,1,0:T(8,128)S(1)}, f32[16,8,8,128]{3,2,1,0:T(8,128)}, u32[]{:S(2)}) copy-start(f32[16,8,8,128]{3,2,1,0:T(8,128)} %copy.97) | copy-start | bytes 1572868
  184.1 9.7 %copy-start.11 = (f32[1024]{0:T(1024)S(1)}, f32[1024]{0:T(1024)}, u32[]{:S(2)}) copy-start(f32[1024]{0:T(1024)} %param.21) | copy-start | bytes 12292
  184.9 13.5 %copy-start.7 = (bf16[64,2048]{1,0:T(8,128)(2,1)S(1)}, bf16[64,2048]{1,0:T(8,128)(2,1)}, u32[]{:S(2)}) copy-start(bf16[64,2048]{1,0:T(8,128)(2,1)} %param.22) | copy-start | bytes 786436
  198.4 5.1 %copy-start.10 = (f32[2048]{0:T(1024)S(1)}, f32[2048]{0:T(1024)}, u32[]{:S(2)}) copy-start(f32[2048]{0:T(1024)} %param.24) | copy-start | bytes 24580
  206.7 48.2 %all-to-all-start.1 = ((bf16[16,16,2048]{2,1,0:T(8,128)(2,1)}), bf16[16,16,2048]{2,1,0:T(8,128)(2,1)S(1)}, u32[]{:S(2)}, u32[]{:S(2)}) async-start(bf16[16,16,2048]{2,1,0:T(8,128)(2,1)} %bitcast.23), calls=%async_computation.1 | async-start | bytes 2097152 | tf_op jit(solution)/shard_map/all_to_all | solution.py:125
  258.3 13.3 %copy-start.13 = (f32[64,2]{0,1:T(2,128)S(1)}, f32[64,2]{0,1:T(2,128)}, u32[]{:S(2)}) copy-start(f32[64,2]{0,1:T(2,128)} %param.26) | copy-start | bytes 1540
  265.4 29.5 %all-to-all-start.2 = ((bf16[16,16,2048]{2,1,0:T(8,128)(2,1)}), bf16[16,16,2048]{2,1,0:T(8,128)(2,1)S(1)}, u32[]{:S(2)}, u32[]{:S(2)}) async-start(bf16[16,16,2048]{2,1,0:T(8,128)(2,1)} %bitcast.30), calls=%async_computation.2 | async-start | bytes 2097152 | tf_op jit(solution)/shard_map/all_to_all | solution.py:140
Sparse Core Ops, SparseCore 0:
  45.6 137.9 all-gather.8
  185.2 18.2 all-gather.4
  205.0 14.6 all-gather.6
where the time goes:
time: 307 us; the launch traced here: 305 us
  waiting for transfers between devices  139 us (45%)
  local copies, waits for them, and re-layouts  59 us (19%)
  other arithmetic  31.8 us (10%)
  starting transfers between devices  30.1 us (10%)
  matrix products  26.9 us (9%)
  between operations  13.8 us (4%)
  blocking collectives  4.13 us (1%)
    all_gather x1, waiting for transfers between devices, carried_in(): gathered = lax.all_gather(part, axis)  91 us
    pad x8, local copies, waits for them, and re-layouts, body(): lax.associative_scan(combine_pair, (jnp.exp(last_log), block_states), axi...  37.1 us
    all_to_all x1, waiting for transfers between devices, body(): lax.all_to_all(outbox.reshape(experts, capacity, width), 'sp', split_axis...  24.6 us
    all_to_all x1, starting transfers between devices, body(): lax.all_to_all(outbox.reshape(experts, capacity, width), 'sp', split_axis...  23.6 us
    all_to_all x1, waiting for transfers between devices, body(): lax.all_to_all(expert_out, 'sp', split_axis=0, concat_axis=0, tiled=True)  23.2 us
    unnamed x37, local copies, waits for them, and re-layouts  15.3 us
    dot_general x1, matrix products, body(): jnp.einsum('ntjd,njdv->ntjv', queries * jnp.exp(cumulative), start_state,...  8.89 us
    add x6, other arithmetic, body(): lax.associative_scan(combine_pair, (jnp.exp(last_log), block_states), axi...  8.53 us
  transfers between devices with their start and end apart: 5, of which 3 were waited for; matrix products, arithmetic and copies ran while one was open for 22% of the time, Pallas kernels for 0%

commit v1 on v0

v1 whole, which is shorter than its diff:
```python
import functools

import jax
import jax.numpy as jnp
from jax import lax
from jax.experimental import pallas as pl
from jax.experimental.pallas import tpu as pltpu
from jax.sharding import PartitionSpec as P

HEAD_DIM = 128
MESH = pl.DeviceIdType.MESH
epsilon = 1e-06
f32 = jnp.float32
bf16 = jnp.bfloat16
NT = (((1,), (1,)), ((), ()))
TN = (((0,), (0,)), ((), ()))


def dot(a, b, dims=(((1,), (0,)), ((), ())), precision=None):
    return lax.dot_general(a, b, dims, precision=precision, preferred_element_type=f32)


def rows_of(index, count):
    return pl.ds(pl.multiple_of(index * count, count), count)


def greet(n):
    me, core = lax.axis_index("sp"), lax.axis_index("tp")
    barrier = pltpu.get_barrier_semaphore()
    pl.semaphore_signal(barrier, inc=1, device_id={"tp": 1 - core}, device_id_type=MESH)

    @pl.loop(1, n)
    def _(r):
        pl.semaphore_signal(
            barrier, inc=1, device_id={"sp": lax.rem(me + r, n)}, device_id_type=MESH
        )

    return barrier


def scan_kernel(
    n, cap,
    query, logit, value, gate, bound, gain, residual, ffn_gain, routing, weight, w_hbm,
    updated_out, outbox_out, combine_out,
    w_out, q_scr, k_scr, ho, st_send, st_recv, dec_send, dec_recv, ret_send, ret_recv,
    mixed, regrouped, proj, w_sem, s_sem, r_sem, ds_sem, dr_sem, bs_sem, br_sem, ms_sem, mr_sem,
):
    me, core = lax.axis_index("sp"), lax.axis_index("tp")
    length, width = query.shape
    heads = width // HEAD_DIM
    piece = width // n
    half = length // 2
    w_copy = pltpu.make_async_copy(w_hbm, w_out, w_sem)
    w_copy.start()
    barrier = greet(n)

    row = lax.broadcasted_iota(jnp.int32, (length, length), 0)
    col = lax.broadcasted_iota(jnp.int32, (length, length), 1)
    causal = row >= col
    tri = causal.astype(f32)
    for h in range(heads):
        c = slice(h * HEAD_DIM, (h + 1) * HEAD_DIM)
        key = (1.0 - bound[:, c]) / (1.0 + jnp.exp(logit[:, c].astype(f32)))
        cum = dot(tri, jnp.log1p(-key), precision=lax.Precision.HIGHEST)
        last = cum[length - 1 :, :]
        mid = 0.5 * last
        q_scr[:, c] = (query[:, c].astype(f32) * jnp.exp(cum - mid)).astype(bf16)
        keys = (key * jnp.exp(mid - cum)).astype(bf16)
        k_scr[:, c] = keys
        st_send[c, :] = (dot(value[:, c], keys, TN) * jnp.exp(mid)).astype(bf16)
        dec_send[h : h + 1, :] = last

    def state_copy(dst, src):
        return pltpu.make_async_remote_copy(
            src_ref=st_send.at[rows_of(dst, piece)], dst_ref=st_recv.at[src],
            send_sem=s_sem.at[dst], recv_sem=r_sem.at[src],
            device_id={"sp": dst}, device_id_type=MESH,
        )

    def decay_copy(dst, src):
        return pltpu.make_async_remote_copy(
            src_ref=dec_send, dst_ref=dec_recv.at[src],
            send_sem=ds_sem.at[dst], recv_sem=dr_sem.at[src],
            device_id={"sp": dst}, device_id_type=MESH,
        )

    def back_copy(dst, src):
        return pltpu.make_async_remote_copy(
            src_ref=ret_send.at[dst], dst_ref=ret_recv.at[rows_of(src, piece)],
            send_sem=bs_sem.at[dst], recv_sem=br_sem.at[src],
            device_id={"sp": dst}, device_id_type=MESH,
        )

    pl.semaphore_wait(barrier, n)

    @pl.loop(1, n)
    def _(r):
        dst = lax.rem(me + r, n)
        decay_copy(dst, me).start()
        state_copy(dst, me).start()

    st_recv[me] = st_send[rows_of(me, piece), :]
    dec_recv[me] = dec_send[...]

    for h in range(heads):
        c = slice(h * HEAD_DIM, (h + 1) * HEAD_DIM)
        scores = jnp.where(causal, dot(q_scr[:, c], k_scr[:, c], NT), 0.0).astype(bf16)
        ho[:, c] = dot(scores, value[:, c])

    slots = n * cap
    count = routing.shape[0]
    expert = lax.broadcasted_iota(jnp.int32, (count, n), 1)
    slot_of = lax.broadcasted_iota(jnp.int32, (count, slots), 1)
    before = (
        lax.broadcasted_iota(jnp.int32, (count, count), 0)
        > lax.broadcasted_iota(jnp.int32, (count, count), 1)
    ).astype(bf16)
    used = jnp.zeros((1, n), f32)
    picks = jnp.zeros((count, slots), f32)
    combine = jnp.zeros((count, slots), f32)
    for k in range(routing.shape[1]):
        hot = (routing[:, k : k + 1] == expert).astype(f32)
        rank = dot(before, hot.astype(bf16)) + used
        used = used + jnp.sum(hot, axis=0, keepdims=True)
        slot = jnp.sum(hot * (rank + expert.astype(f32) * cap), axis=1, keepdims=True)
        mine = slot.astype(jnp.int32) == slot_of
        picks = jnp.where(mine, 1.0, picks)
        combine = jnp.where(mine, weight[:, k : k + 1], combine)
    combine_out[...] = combine

    @pl.loop(1, n)
    def _(r):
        src = lax.rem(me + r, n)
        decay_copy(me, src).wait_recv()
        state_copy(me, src).wait_recv()

    my_head = me * piece // HEAD_DIM

    def prefix(p, acc):
        last = dec_recv[p, pl.ds(my_head, 1), :]
        ret_send[p] = (acc * jnp.exp(0.5 * last)).astype(bf16)
        return acc * jnp.exp(last) + st_recv[p].astype(f32)

    lax.fori_loop(0, n, prefix, jnp.zeros((piece, HEAD_DIM), f32))

    @pl.loop(1, n)
    def _(r):
        back_copy(lax.rem(me + r, n), me).start()

    ret_recv[rows_of(me, piece), :] = ret_send[me]

    @pl.loop(1, n)
    def _(r):
        back_copy(me, lax.rem(me + r, n)).wait_recv()

    for h in range(heads):
        c = slice(h * HEAD_DIM, (h + 1) * HEAD_DIM)
        out = ho[:, c] + dot(q_scr[:, c], ret_recv[c, :], NT)
        out = out * lax.rsqrt(jnp.mean(out * out, axis=1, keepdims=True) + epsilon)
        g = gate[:, c].astype(f32)
        out = (out * gain[:, c] * (g / (1.0 + jnp.exp(-g)))).astype(bf16)
        mixed[0, :, c] = out[:half]
        mixed[1, :, c] = out[half:]

    swap = pltpu.make_async_remote_copy(
        src_ref=mixed.at[1 - core], dst_ref=regrouped,
        send_sem=ms_sem, recv_sem=mr_sem,
        device_id={"tp": 1 - core}, device_id_type=MESH,
    )
    swap.start()
    w_copy.wait()
    tile = 512
    total = w_out.shape[1]

    def project(which, source, first):
        @pl.loop(0, total // tile)
        def _(j):
            cols = pl.ds(pl.multiple_of(j * tile, tile), tile)
            part = dot(source, w_out[rows_of(which, width), cols])
            proj[:, cols] = part if first else proj[:, cols] + part

    project(core, mixed[core], True)
    swap.wait()
    project(1 - core, regrouped[...], False)
    updated = (residual[...].astype(f32) + proj[...]).astype(bf16)
    updated_out[...] = updated
    updated = updated.astype(f32)
    normed = (
        updated
        * lax.rsqrt(jnp.mean(updated * updated, axis=1, keepdims=True) + epsilon)
        * ffn_gain[...]
    ).astype(bf16)
    outbox_out[...] = dot(picks.astype(bf16), normed, TN).astype(bf16)

    @pl.loop(1, n)
    def _(r):
        dst = lax.rem(me + r, n)
        decay_copy(dst, me).wait_send()
        state_copy(dst, me).wait_send()
        back_copy(dst, me).wait_send()


def expert_kernel(
    n, cap,
    outbox, updated, combine, g_hbm, u_hbm, d_hbm,
    out,
    wg, wu, wd, arrived, hidden, result, returned,
    l_sem, ps_sem, pr_sem, s_sem, r_sem, bs_sem, br_sem,
):
    me, core = lax.axis_index("sp"), lax.axis_index("tp")
    barrier = greet(n)
    homes = ((g_hbm, wg), (u_hbm, wu), (d_hbm, wd))
    local = [
        pltpu.make_async_copy(src.at[0], dst.at[0], l_sem.at[i])
        for i, (src, dst) in enumerate(homes)
    ]
    for copy in local:
        copy.start()

    def send_copy(dst, src):
        return pltpu.make_async_remote_copy(
            src_ref=outbox.at[rows_of(dst, cap)], dst_ref=arrived.at[rows_of(src, cap)],
            send_sem=s_sem.at[dst], recv_sem=r_sem.at[src],
            device_id={"sp": dst}, device_id_type=MESH,
        )

    def back_copy(dst, src):
        return pltpu.make_async_remote_copy(
            src_ref=result.at[rows_of(dst, cap)], dst_ref=returned.at[rows_of(src, cap)],
            send_sem=bs_sem.at[dst], recv_sem=br_sem.at[src],
            device_id={"sp": dst}, device_id_type=MESH,
        )

    pl.semaphore_wait(barrier, n)

    @pl.loop(1, n)
    def _(r):
        send_copy(lax.rem(me + r, n), me).start()

    peer = [
        pltpu.make_async_remote_copy(
            src_ref=src.at[0], dst_ref=dst.at[1],
            send_sem=ps_sem.at[i], recv_sem=pr_sem.at[i],
            device_id={"tp": 1 - core}, device_id_type=MESH,
        )
        for i, (src, dst) in enumerate(homes)
    ]
    for copy in peer:
        copy.start()
    arrived[rows_of(me, cap), :] = outbox[rows_of(me, cap), :]
    for copy in local:
        copy.wait()
    for copy in peer:
        copy.wait()

    @pl.loop(1, n)
    def _(r):
        send_copy(me, lax.rem(me + r, n)).wait_recv()

    inner = wg.shape[2]
    tile = 256
    for s in range(2):

        @pl.loop(0, inner // tile)
        def _(j):
            cols = rows_of(j, tile)
            g = dot(arrived[...], wg[s, :, cols])
            u = dot(arrived[...], wu[s, :, cols])
            hidden[s, :, cols] = (g / (1.0 + jnp.exp(-g)) * u).astype(bf16)

    wide = 512

    @pl.loop(0, wd.shape[2] // wide)
    def _(j):
        cols = rows_of(j, wide)
        result[:, cols] = (
            dot(hidden[0], wd[0, :, cols]) + dot(hidden[1], wd[1, :, cols])
        ).astype(bf16)

    @pl.loop(1, n)
    def _(r):
        back_copy(lax.rem(me + r, n), me).start()

    returned[rows_of(me, cap), :] = result[rows_of(me, cap), :]
    high = combine[...].astype(bf16)
    low = (combine[...] - high.astype(f32)).astype(bf16)

    @pl.loop(1, n)
    def _(r):
        back_copy(me, lax.rem(me + r, n)).wait_recv()

    @pl.loop(0, out.shape[1] // wide)
    def _(j):
        cols = rows_of(j, wide)
        back = returned[:, cols]
        out[:, cols] = (
            updated[:, cols].astype(f32) + (dot(high, back) + dot(low, back))
        ).astype(bf16)

    @pl.loop(1, n)
    def _(r):
        dst = lax.rem(me + r, n)
        send_copy(dst, me).wait_send()
        back_copy(dst, me).wait_send()


def solution(mesh):
    n = mesh.shape["sp"]
    vmem = pl.BlockSpec(memory_space=pltpu.VMEM)
    hbm = pl.BlockSpec(memory_space=pl.ANY)
    dma = pltpu.SemaphoreType.DMA

    def body(
        query, forget_logit, value, out_gate, lower_bound, head_gain, residual_in, w_out,
        ffn_gain, routing, route_weight, expert_gate, expert_up, expert_down,
    ):
        length, width = query.shape
        heads = width // HEAD_DIM
        half, model = residual_in.shape
        cap = 2 * half * routing.shape[1] // n
        cap = -(-cap // 16) * 16
        slots = n * cap
        piece = width // n
        updated, outbox, combine = pl.pallas_call(
            functools.partial(scan_kernel, n, cap),
            out_shape=(
                jax.ShapeDtypeStruct((half, model), bf16),
                jax.ShapeDtypeStruct((slots, model), bf16),
                jax.ShapeDtypeStruct((half, slots), f32),
            ),
            in_specs=[vmem] * 10 + [hbm],
            out_specs=(vmem, vmem, vmem),
            scratch_shapes=[
                pltpu.VMEM(w_out.shape, bf16),
                pltpu.VMEM((length, width), bf16),
                pltpu.VMEM((length, width), bf16),
                pltpu.VMEM((length, width), f32),
                pltpu.VMEM((width, HEAD_DIM), bf16),
                pltpu.VMEM((n, piece, HEAD_DIM), bf16),
                pltpu.VMEM((heads, HEAD_DIM), f32),
                pltpu.VMEM((n, heads, HEAD_DIM), f32),
                pltpu.VMEM((n, piece, HEAD_DIM), bf16),
                pltpu.VMEM((width, HEAD_DIM), bf16),
                pltpu.VMEM((2, half, width), bf16),
                pltpu.VMEM((half, width), bf16),
                pltpu.VMEM((half, model), f32),
                dma, dma((n,)), dma((n,)), dma((n,)), dma((n,)), dma((n,)), dma((n,)), dma, dma,
            ],
            compiler_params=pltpu.CompilerParams(
                collective_id=0, has_side_effects=True, vmem_limit_bytes=50 << 20
            ),
        )(
            query, forget_logit, value, out_gate, lower_bound[None], head_gain[None],
            residual_in, ffn_gain[None], routing, route_weight, w_out,
        )
        inner = expert_gate.shape[2]
        return pl.pallas_call(
            functools.partial(expert_kernel, n, cap),
            out_shape=jax.ShapeDtypeStruct((half, model), bf16),
            in_specs=[vmem] * 3 + [hbm] * 3,
            out_specs=vmem,
            scratch_shapes=[
                pltpu.VMEM((2, model, inner), bf16),
                pltpu.VMEM((2, model, inner), bf16),
                pltpu.VMEM((2, inner, model), bf16),
                pltpu.VMEM((slots, model), bf16),
                pltpu.VMEM((2, slots, inner), bf16),
                pltpu.VMEM((slots, model), bf16),
                pltpu.VMEM((slots, model), bf16),
                dma((3,)), dma((3,)), dma((3,)),
                dma((n,)), dma((n,)), dma((n,)), dma((n,)),
            ],
            compiler_params=pltpu.CompilerParams(
                collective_id=1, has_side_effects=True, vmem_limit_bytes=60 << 20
            ),
        )(outbox, updated, combine, expert_gate, expert_up, expert_down)

    placed = (
        P("sp", "tp"), P("sp", "tp"), P("sp", "tp"), P("sp", "tp"), P("tp"), P("tp"),
        P(("sp", "tp"), None), P(), P(), P(("sp", "tp"), None), P(("sp", "tp"), None),
        P("sp", None, "tp"), P("sp", None, "tp"), P("sp", "tp", None),
    )
    return jax.shard_map(
        body, mesh=mesh, in_specs=placed, out_specs=P(("sp", "tp"), None), check_vma=False
    )
```

time: 307 us -> 95 us (0.31)
  the two profiles are of different devices: /device:TPU:0 before, /device:TPU:28 now
where the time goes in v1:
time: 95 us; the launch traced here: 94.5 us
  Pallas kernels  82.2 us (87%)
  local copies, waits for them, and re-layouts  12.3 us (13%)
    pallas_call x1, Pallas kernels, body(): pl.pallas_call(functools.partial(expert_kernel, n, cap), out_shape=jax.Sh...  58.1 us
    pallas_call x1, Pallas kernels, body(): pl.pallas_call(functools.partial(scan_kernel, n, cap), out_shape=(jax.Sha...  24.1 us
    unnamed x25, local copies, waits for them, and re-layouts  12.3 us

profile of v1, /device:TPU:28, one launch (start us, length us, event | category | flops | bytes accessed | tf_op | source)
XLA Modules:
  0.0 94.5 jit_solution(5097443727088828382)
XLA Ops:
  0.0 0.8 copy.15.routing
  0.8 0.8 copy.16.weight
  1.5 0.0 copy-start.1
  1.5 0.9 %copy-done.1 = bf16[128,1024]{1,0:T(8,128)(2,1)S(1)} copy-done((bf16[128,1024]{1,0:T(8,128)(2,1)S(1)}, bf16[128,1024]{1,0:T(8,128)(2,1)}, u32[]{:S(2)}) %copy-start.1) | copy-done | bytes 262168
  2.5 0.0 copy-start.2
  2.5 0.9 %copy-done.2 = bf16[128,1024]{1,0:T(8,128)(2,1)S(1)} copy-done((bf16[128,1024]{1,0:T(8,128)(2,1)S(1)}, bf16[128,1024]{1,0:T(8,128)(2,1)}, u32[]{:S(2)}) %copy-start.2) | copy-done | bytes 262168
  3.4 0.0 copy-start.3
  3.4 0.9 %copy-done.3 = bf16[128,1024]{1,0:T(8,128)(2,1)S(1)} copy-done((bf16[128,1024]{1,0:T(8,128)(2,1)S(1)}, bf16[128,1024]{1,0:T(8,128)(2,1)}, u32[]{:S(2)}) %copy-start.3) | copy-done | bytes 262168
  4.4 0.0 copy-start.4
  4.4 0.9 %copy-done.4 = bf16[128,1024]{1,0:T(8,128)(2,1)S(1)} copy-done((bf16[128,1024]{1,0:T(8,128)(2,1)S(1)}, bf16[128,1024]{1,0:T(8,128)(2,1)}, u32[]{:S(2)}) %copy-start.4) | copy-done | bytes 262168
  5.3 0.0 copy-start.5
  5.3 0.9 %copy-done.5 = bf16[64,2048]{1,0:T(8,128)(2,1)S(1)} copy-done((bf16[64,2048]{1,0:T(8,128)(2,1)S(1)}, bf16[64,2048]{1,0:T(8,128)(2,1)}, u32[]{:S(2)}) %copy-start.5) | copy-done | bytes 262168
  6.3 0.0 copy-start.8
  6.3 0.7 copy-done.8
  7.0 0.0 copy-start.9
  7.0 0.7 copy-done.9
  7.7 0.0 copy-start.10
  7.7 0.7 copy-done.10
  8.4 24.1 %shard_map.136 = (bf16[64,2048]{1,0:T(8,128)(2,1)S(1)}, bf16[256,2048]{1,0:T(8,128)(2,1)S(1)}, f32[64,256]{1,0:T(8,128)S(1)}) custom-call(bf16[128,1024]{1,0:T(8,128)(2,1)S(1)} %copy-done.1, bf16[128,1024]{1,0:T(8,128)(2,1)S(1)} %copy-done.2, bf16[128,1024]{1,0:T(8,128)(2,1)S(1)} %copy-done.3, bf16[128,1024]{1,0:T(8,128)(2,1)S(1)} %copy-done.4, ...), custom_call_target="tpu_custom_call" | custom-call | tf_op jit(solution)/shard_map/pallas_call | solution.py:324
  32.4 0.0 copy-start
  32.4 1.0 %copy-done = bf16[256,2048]{1,0:T(8,128)(2,1)} copy-done((bf16[256,2048]{1,0:T(8,128)(2,1)}, bf16[256,2048]{1,0:T(8,128)(2,1)S(1)}, u32[]{:S(2)}) %copy-start) | copy-done | bytes 1048600
  33.4 0.0 copy-start.6
  33.4 0.7 copy-done.6
  34.1 0.0 copy-start.7
  34.1 0.6 copy-done.7
  34.7 58.1 %shard_map.137 = bf16[64,2048]{1,0:T(8,128)(2,1)} custom-call(bf16[256,2048]{1,0:T(8,128)(2,1)} %copy-done, bf16[64,2048]{1,0:T(8,128)(2,1)} %copy-done.6, f32[64,256]{1,0:T(8,128)} %copy-done.7, bf16[1,2048,512]{2,1,0:T(8,128)(2,1)} %g_hbm.1, bf16[1,2048,512]{2,1,0:T(8,128)(2,1)} %u_hbm.1, bf16[1,512,2048]{2,1,0:T(8,128)(2,1)} %d_hbm.1), custom_call_target="tpu_custom_call" | custom-call | tf_op jit(solution)/shard_map/pallas_call | solution.py:357
  92.9 1.7 %copy.18 = bf16[64,2048]{1,0:T(8,128)(2,1)} copy(bf16[64,2048]{1,0:T(8,128)(2,1)} %shard_map.137) | data formatting | bytes 524288
Async XLA Ops:
  1.5 0.9 %copy-start.1 = (bf16[128,1024]{1,0:T(8,128)(2,1)S(1)}, bf16[128,1024]{1,0:T(8,128)(2,1)}, u32[]{:S(2)}) copy-start(bf16[128,1024]{1,0:T(8,128)(2,1)} %query.1) | copy-start | bytes 786436
  2.5 0.9 %copy-start.2 = (bf16[128,1024]{1,0:T(8,128)(2,1)S(1)}, bf16[128,1024]{1,0:T(8,128)(2,1)}, u32[]{:S(2)}) copy-start(bf16[128,1024]{1,0:T(8,128)(2,1)} %logit.1) | copy-start | bytes 786436
  3.4 0.9 %copy-start.3 = (bf16[128,1024]{1,0:T(8,128)(2,1)S(1)}, bf16[128,1024]{1,0:T(8,128)(2,1)}, u32[]{:S(2)}) copy-start(bf16[128,1024]{1,0:T(8,128)(2,1)} %value.1) | copy-start | bytes 786436
  4.4 0.9 %copy-start.4 = (bf16[128,1024]{1,0:T(8,128)(2,1)S(1)}, bf16[128,1024]{1,0:T(8,128)(2,1)}, u32[]{:S(2)}) copy-start(bf16[128,1024]{1,0:T(8,128)(2,1)} %gate.1) | copy-start | bytes 786436
  5.3 0.9 %copy-start.5 = (bf16[64,2048]{1,0:T(8,128)(2,1)S(1)}, bf16[64,2048]{1,0:T(8,128)(2,1)}, u32[]{:S(2)}) copy-start(bf16[64,2048]{1,0:T(8,128)(2,1)} %residual.1) | copy-start | bytes 786436
  6.3 0.7 copy-start.8
  7.0 0.7 copy-start.9
  7.7 0.7 copy-start.10
  32.4 1.0 %copy-start = (bf16[256,2048]{1,0:T(8,128)(2,1)}, bf16[256,2048]{1,0:T(8,128)(2,1)S(1)}, u32[]{:S(2)}) copy-start(bf16[256,2048]{1,0:T(8,128)(2,1)S(1)} %get-tuple-element.8.outbox) | copy-start | bytes 3145732
  33.4 0.7 copy-start.6
  34.1 0.6 copy-start.7

commit v2 on v1

v2 whole, which is shorter than its diff:
```python
import functools

import jax
import jax.numpy as jnp
from jax import lax
from jax.experimental import pallas as pl
from jax.experimental.pallas import tpu as pltpu
from jax.sharding import PartitionSpec as P

HEAD_DIM = 128
MESH = pl.DeviceIdType.MESH
epsilon = 1e-06
f32 = jnp.float32
bf16 = jnp.bfloat16
NT = (((1,), (1,)), ((), ()))
TN = (((0,), (0,)), ((), ()))


def dot(a, b, dims=(((1,), (0,)), ((), ())), precision=None):
    return lax.dot_general(a, b, dims, precision=precision, preferred_element_type=f32)


def rows_of(index, count):
    return pl.ds(pl.multiple_of(index * count, count), count)


def greet(n):
    me, core = lax.axis_index("sp"), lax.axis_index("tp")
    barrier = pltpu.get_barrier_semaphore()
    pl.semaphore_signal(barrier, inc=1, device_id={"tp": 1 - core}, device_id_type=MESH)

    @pl.loop(1, n)
    def _(r):
        pl.semaphore_signal(
            barrier, inc=1, device_id={"sp": lax.rem(me + r, n)}, device_id_type=MESH
        )

    return barrier


def partner(me, r):
    other = me
    step = 1
    while step <= r:
        if r & step:
            other = other + step * (1 - 2 * (me // step % 2))
        step *= 2
    return other


def layer_kernel(
    n, cap,
    query_h, logit_h, value_h, gate_h, bound_h, gain_h, residual_h, ffn_gain_h, routing_h,
    weight_h, w_hbm, g_hbm, u_hbm, d_hbm,
    layer_out,
    query, logit, value, gate, bound, gain, residual, ffn_gain, routing, weight,
    w_out, q_scr, k_scr, ho, st_send, st_recv, dec_send, dec_recv, ret_send, ret_recv,
    mixed, regrouped, proj,
    wg, wu, wd, outbox, arrived, hidden, result, returned,
    in_sem, w_sem, s_sem, r_sem, ds_sem, dr_sem, bs_sem, br_sem, ms_sem, mr_sem,
    l_sem, ps_sem, pr_sem, xs_sem, xr_sem, ys_sem, yr_sem,
):
    me, core = lax.axis_index("sp"), lax.axis_index("tp")
    length, width = query.shape
    heads = width // HEAD_DIM
    piece = width // n
    half = length // 2
    moves = [
        pltpu.make_async_copy(src, dst, in_sem.at[i])
        for i, (src, dst) in enumerate((
            (logit_h, logit), (bound_h, bound), (query_h, query), (value_h, value),
            (routing_h, routing), (weight_h, weight), (gate_h, gate), (gain_h, gain),
            (residual_h, residual), (ffn_gain_h, ffn_gain),
        ))
    ]
    for move in moves:
        move.start()
    barrier = greet(n)
    w_copy = pltpu.make_async_copy(w_hbm, w_out, w_sem)
    homes = ((g_hbm, wg), (u_hbm, wu), (d_hbm, wd))
    local = [
        pltpu.make_async_copy(src.at[0], dst.at[0], l_sem.at[i])
        for i, (src, dst) in enumerate(homes)
    ]
    peer = [
        pltpu.make_async_remote_copy(
            src_ref=src.at[0], dst_ref=dst.at[1],
            send_sem=ps_sem.at[i], recv_sem=pr_sem.at[i],
            device_id={"tp": 1 - core}, device_id_type=MESH,
        )
        for i, (src, dst) in enumerate(homes)
    ]
    for move in moves[:4]:
        move.wait()
    w_copy.start()

    row = lax.broadcasted_iota(jnp.int32, (length, length), 0)
    col = lax.broadcasted_iota(jnp.int32, (length, length), 1)
    causal = row >= col
    tri = causal.astype(f32)
    for h in range(heads):
        c = slice(h * HEAD_DIM, (h + 1) * HEAD_DIM)
        key = (1.0 - bound[:, c]) / (1.0 + jnp.exp(logit[:, c].astype(f32)))
        cum = dot(tri, jnp.log1p(-key), precision=lax.Precision.HIGHEST)
        last = cum[length - 1 :, :]
        mid = 0.5 * last
        q_scr[:, c] = (query[:, c].astype(f32) * jnp.exp(cum - mid)).astype(bf16)
        keys = (key * jnp.exp(mid - cum)).astype(bf16)
        k_scr[:, c] = keys
        st_send[c, :] = (dot(value[:, c], keys, TN) * jnp.exp(mid)).astype(bf16)
        dec_send[h : h + 1, :] = last
        if h == (heads - 1) // 2:
            pl.semaphore_wait(barrier, n)
            for copy in peer + local:
                copy.start()

    def state_copy(dst, src):
        return pltpu.make_async_remote_copy(
            src_ref=st_send.at[rows_of(dst, piece)], dst_ref=st_recv.at[src],
            send_sem=s_sem.at[dst], recv_sem=r_sem.at[src],
            device_id={"sp": dst}, device_id_type=MESH,
        )

    def decay_copy(dst, src):
        return pltpu.make_async_remote_copy(
            src_ref=dec_send, dst_ref=dec_recv.at[src],
            send_sem=ds_sem.at[dst], recv_sem=dr_sem.at[src],
            device_id={"sp": dst}, device_id_type=MESH,
        )

    def back_copy(dst, src):
        return pltpu.make_async_remote_copy(
            src_ref=ret_send.at[dst], dst_ref=ret_recv.at[rows_of(src, piece)],
            send_sem=bs_sem.at[dst], recv_sem=br_sem.at[src],
            device_id={"sp": dst}, device_id_type=MESH,
        )

    @pl.loop(1, n)
    def _(r):
        dst = lax.rem(me + r, n)
        decay_copy(dst, me).start()
        state_copy(dst, me).start()

    st_recv[me] = st_send[rows_of(me, piece), :]
    dec_recv[me] = dec_send[...]

    for h in range(heads):
        c = slice(h * HEAD_DIM, (h + 1) * HEAD_DIM)
        scores = jnp.where(causal, dot(q_scr[:, c], k_scr[:, c], NT), 0.0).astype(bf16)
        ho[:, c] = dot(scores, value[:, c])

    slots = n * cap
    for move in moves[4:]:
        move.wait()
    top, count = routing.shape
    eye = lax.broadcasted_iota(jnp.int32, (count, count), 0) == lax.broadcasted_iota(
        jnp.int32, (count, count), 1
    )

    def column(line):
        return jnp.sum(jnp.where(eye, line, 0.0), axis=1, keepdims=True)

    expert = lax.broadcasted_iota(jnp.int32, (count, n), 1).astype(f32)
    slot_of = lax.broadcasted_iota(jnp.int32, (count, slots), 1)
    before = (
        lax.broadcasted_iota(jnp.int32, (count, count), 0)
        > lax.broadcasted_iota(jnp.int32, (count, count), 1)
    ).astype(bf16)
    used = jnp.zeros((1, n), f32)
    picks = jnp.zeros((count, slots), f32)
    combine = jnp.zeros((count, slots), f32)
    for k in range(top):
        hot = (column(routing[k : k + 1, :].astype(f32)) == expert).astype(f32)
        rank = dot(before, hot.astype(bf16)) + used
        used = used + jnp.sum(hot, axis=0, keepdims=True)
        slot = jnp.sum(hot * (rank + expert * cap), axis=1, keepdims=True)
        mine = slot.astype(jnp.int32) == slot_of
        picks = jnp.where(mine, 1.0, picks)
        combine = jnp.where(mine, column(weight[k : k + 1, :]), combine)
    high = combine.astype(bf16)
    both = jnp.concatenate([high, (combine - high.astype(f32)).astype(bf16)], axis=0)

    @pl.loop(1, n)
    def _(r):
        src = lax.rem(me + r, n)
        decay_copy(me, src).wait_recv()
        state_copy(me, src).wait_recv()

    my_head = me * piece // HEAD_DIM

    def prefix(p, acc):
        last = dec_recv[p, pl.ds(my_head, 1), :]
        ret_send[p] = (acc * jnp.exp(0.5 * last)).astype(bf16)
        return acc * jnp.exp(last) + st_recv[p].astype(f32)

    lax.fori_loop(0, n, prefix, jnp.zeros((piece, HEAD_DIM), f32))

    @pl.loop(1, n)
    def _(r):
        back_copy(lax.rem(me + r, n), me).start()

    ret_recv[rows_of(me, piece), :] = ret_send[me]

    @pl.loop(1, n)
    def _(r):
        back_copy(me, lax.rem(me + r, n)).wait_recv()

    for h in range(heads):
        c = slice(h * HEAD_DIM, (h + 1) * HEAD_DIM)
        out = ho[:, c] + dot(q_scr[:, c], ret_recv[c, :], NT)
        out = out * lax.rsqrt(jnp.mean(out * out, axis=1, keepdims=True) + epsilon)
        g = gate[:, c].astype(f32)
        out = (out * gain[:, c] * (g / (1.0 + jnp.exp(-g)))).astype(bf16)
        mixed[0, :, c] = out[:half]
        mixed[1, :, c] = out[half:]

    swap = pltpu.make_async_remote_copy(
        src_ref=mixed.at[1 - core], dst_ref=regrouped,
        send_sem=ms_sem, recv_sem=mr_sem,
        device_id={"tp": 1 - core}, device_id_type=MESH,
    )
    swap.start()
    w_copy.wait()
    tile = 512
    total = w_out.shape[1]

    def project(which, source, first):
        @pl.loop(0, total // tile)
        def _(j):
            cols = pl.ds(pl.multiple_of(j * tile, tile), tile)
            part = dot(source, w_out[rows_of(which, width), cols])
            proj[:, cols] = part if first else proj[:, cols] + part

    project(core, mixed[core], True)
    swap.wait()
    project(1 - core, regrouped[...], False)
    updated = (residual[...].astype(f32) + proj[...]).astype(bf16)
    updated = updated.astype(f32)
    proj[...] = updated
    normed = (
        updated
        * lax.rsqrt(jnp.mean(updated * updated, axis=1, keepdims=True) + epsilon)
        * ffn_gain[...]
    ).astype(bf16)
    outbox[...] = dot(picks.astype(bf16), normed, TN).astype(bf16)

    sets = [
        [r for r in range(n - 1, -1, -1) if (r ^ (r >> 1)) & 1 == which] for which in range(2)
    ]
    place = {r: i for i, r in enumerate(sets[0] + sets[1])}

    def block(r):
        return pl.ds(place[r] * cap, cap)

    def send_copy(r):
        return pltpu.make_async_remote_copy(
            src_ref=outbox.at[rows_of(partner(me, r), cap)], dst_ref=arrived.at[block(r)],
            send_sem=xs_sem.at[r], recv_sem=xr_sem.at[r],
            device_id={"sp": partner(me, r)}, device_id_type=MESH,
        )

    def answer_copy(r):
        return pltpu.make_async_remote_copy(
            src_ref=result.at[block(r)], dst_ref=returned.at[rows_of(me, cap)],
            send_sem=ys_sem.at[r], recv_sem=yr_sem.at[r],
            device_id={"sp": partner(me, r)}, device_id_type=MESH,
        )

    def answer_from(r):
        return pltpu.make_async_remote_copy(
            src_ref=result.at[block(r)], dst_ref=returned.at[rows_of(partner(me, r), cap)],
            send_sem=ys_sem.at[r], recv_sem=yr_sem.at[r],
            device_id={"sp": partner(me, r)}, device_id_type=MESH,
        )

    for r in sets[0] + sets[1]:
        if r:
            send_copy(r).start()
    arrived[block(0), :] = outbox[rows_of(me, cap), :]
    for copy in peer + local:
        copy.wait()
    inner = wg.shape[2]
    narrow = 256
    first = 0
    for group in sets:
        for r in group:
            if r:
                send_copy(r).wait_recv()
        part = slice(first, first + len(group) * cap)
        first = first + len(group) * cap
        for s in range(2):

            @pl.loop(0, inner // narrow)
            def _(j):
                cols = rows_of(j, narrow)
                g = dot(arrived[part, :], wg[s, :, cols])
                u = dot(arrived[part, :], wu[s, :, cols])
                hidden[s, part, cols] = (g / (1.0 + jnp.exp(-g)) * u).astype(bf16)

        @pl.loop(0, total // tile)
        def _(j):
            cols = rows_of(j, tile)
            result[part, cols] = (
                dot(hidden[0, part, :], wd[0, :, cols]) + dot(hidden[1, part, :], wd[1, :, cols])
            ).astype(bf16)

        for r in group:
            if r:
                answer_copy(r).start()

    returned[rows_of(me, cap), :] = result[block(0), :]
    for r in sets[0] + sets[1]:
        if r:
            answer_from(r).wait_recv()

    @pl.loop(0, total // tile)
    def _(j):
        cols = rows_of(j, tile)
        back = dot(both, returned[:, cols])
        layer_out[:, cols] = (proj[:, cols] + (back[:count] + back[count:])).astype(bf16)

    @pl.loop(1, n)
    def _(r):
        dst = lax.rem(me + r, n)
        decay_copy(dst, me).wait_send()
        state_copy(dst, me).wait_send()
        back_copy(dst, me).wait_send()

    for r in range(1, n):
        send_copy(r).wait_send()
        answer_copy(r).wait_send()


def solution(mesh):
    n = mesh.shape["sp"]
    vmem = pl.BlockSpec(memory_space=pltpu.VMEM)
    hbm = pl.BlockSpec(memory_space=pl.ANY)
    dma = pltpu.SemaphoreType.DMA

    def body(
        query, forget_logit, value, out_gate, lower_bound, head_gain, residual_in, w_out,
        ffn_gain, routing, route_weight, expert_gate, expert_up, expert_down,
    ):
        length, width = query.shape
        heads = width // HEAD_DIM
        half, model = residual_in.shape
        cap = 2 * half * routing.shape[1] // n
        cap = -(-cap // 16) * 16
        slots = n * cap
        piece = width // n
        inner = expert_gate.shape[2]
        top = routing.shape[1]
        return pl.pallas_call(
            functools.partial(layer_kernel, n, cap),
            out_shape=jax.ShapeDtypeStruct((half, model), bf16),
            in_specs=[hbm] * 14,
            out_specs=vmem,
            scratch_shapes=[
                pltpu.VMEM((length, width), bf16),
                pltpu.VMEM((length, width), bf16),
                pltpu.VMEM((length, width), bf16),
                pltpu.VMEM((length, width), bf16),
                pltpu.VMEM((1, width), f32),
                pltpu.VMEM((1, width), f32),
                pltpu.VMEM((half, model), bf16),
                pltpu.VMEM((1, model), f32),
                pltpu.VMEM((top, half), jnp.int32),
                pltpu.VMEM((top, half), f32),
                pltpu.VMEM(w_out.shape, bf16),
                pltpu.VMEM((length, width), bf16),
                pltpu.VMEM((length, width), bf16),
                pltpu.VMEM((length, width), f32),
                pltpu.VMEM((width, HEAD_DIM), bf16),
                pltpu.VMEM((n, piece, HEAD_DIM), bf16),
                pltpu.VMEM((heads, HEAD_DIM), f32),
                pltpu.VMEM((n, heads, HEAD_DIM), f32),
                pltpu.VMEM((n, piece, HEAD_DIM), bf16),
                pltpu.VMEM((width, HEAD_DIM), bf16),
                pltpu.VMEM((2, half, width), bf16),
                pltpu.VMEM((half, width), bf16),
                pltpu.VMEM((half, model), f32),
                pltpu.VMEM((2, model, inner), bf16),
                pltpu.VMEM((2, model, inner), bf16),
                pltpu.VMEM((2, inner, model), bf16),
                pltpu.VMEM((slots, model), bf16),
                pltpu.VMEM((slots, model), bf16),
                pltpu.VMEM((2, slots, inner), bf16),
                pltpu.VMEM((slots, model), bf16),
                pltpu.VMEM((slots, model), bf16),
                dma((10,)), dma, dma((n,)), dma((n,)), dma((n,)), dma((n,)), dma((n,)), dma((n,)),
                dma, dma, dma((3,)), dma((3,)), dma((3,)),
                dma((n,)), dma((n,)), dma((n,)), dma((n,)),
            ],
            compiler_params=pltpu.CompilerParams(
                collective_id=0, has_side_effects=True, vmem_limit_bytes=60 << 20
            ),
        )(
            query, forget_logit, value, out_gate, lower_bound[None], head_gain[None],
            residual_in, ffn_gain[None], routing.T, route_weight.T, w_out,
            expert_gate, expert_up, expert_down,
        )

    placed = (
        P("sp", "tp"), P("sp", "tp"), P("sp", "tp"), P("sp", "tp"), P("tp"), P("tp"),
        P(("sp", "tp"), None), P(), P(), P(("sp", "tp"), None), P(("sp", "tp"), None),
        P("sp", None, "tp"), P("sp", None, "tp"), P("sp", "tp", None),
    )
    return jax.shard_map(
        body, mesh=mesh, in_specs=placed, out_specs=P(("sp", "tp"), None), check_vma=False
    )
```

time: 95 us -> 80.8 us (0.85)
  the two profiles are of different devices: /device:TPU:28 before, /device:TPU:0 now
where the time goes in v2:
time: 80.8 us; the launch traced here: 80.7 us
  Pallas kernels  79 us (98%)
  local copies, waits for them, and re-layouts  1.67 us (2%)
    pallas_call x1, Pallas kernels, body(): pl.pallas_call(functools.partial(layer_kernel, n, cap), out_shape=jax.Sha...  79 us
    unnamed x1, local copies, waits for them, and re-layouts  1.67 us

profile of v2, /device:TPU:0, one launch (start us, length us, event | category | flops | bytes accessed | tf_op | source)
XLA Modules:
  0.0 80.7 jit_solution(5430928868187195582)
XLA Ops:
  0.0 79.0 %shard_map.136 = bf16[64,2048]{1,0:T(8,128)(2,1)} custom-call(bf16[128,1024]{1,0:T(8,128)(2,1)} %query_h.1, bf16[128,1024]{1,0:T(8,128)(2,1)} %logit_h.1, bf16[128,1024]{1,0:T(8,128)(2,1)} %value_h.1, bf16[128,1024]{1,0:T(8,128)(2,1)} %gate_h.1, f32[1,1024]{1,0:T(1,128)} %bitcast.6, f32[1,1024]{1,0:T(1,128)} %bitcast.7, bf16[64,2048]{1,0:T(8,128)(2,1)} %residual_h.1, ...), custom_call_target="tpu_custom_call" | custom-call | tf_op jit(solution)/shard_map/pallas_call | solution.py:353
  79.0 1.7 %copy.16 = bf16[64,2048]{1,0:T(8,128)(2,1)} copy(bf16[64,2048]{1,0:T(8,128)(2,1)} %shard_map.136) | data formatting | bytes 524288

commit v3 on v2

--- a/solution.py
+++ b/solution.py
@@ -63,7 +63,8 @@
     me, core = lax.axis_index("sp"), lax.axis_index("tp")
     length, width = query.shape
     heads = width // HEAD_DIM
-    piece = width // n
+    groups, piece = st_recv.shape[0], st_recv.shape[2]
+    per = heads // groups
     half = length // 2
     moves = [
         pltpu.make_async_copy(src, dst, in_sem.at[i])
@@ -98,6 +99,39 @@
     col = lax.broadcasted_iota(jnp.int32, (length, length), 1)
     causal = row >= col
     tri = causal.astype(f32)
+    def owned(g, index):
+        return pl.ds(pl.multiple_of(g * per * HEAD_DIM + index * piece, piece), piece)
+
+    def state_copy(g, r):
+        return pltpu.make_async_remote_copy(
+            src_ref=st_send.at[owned(g, partner(me, r))], dst_ref=st_recv.at[g, r],
+            send_sem=s_sem.at[g, r], recv_sem=r_sem.at[g, r],
+            device_id={"sp": partner(me, r)}, device_id_type=MESH,
+        )
+
+    def decay_copy(g, r):
+        return pltpu.make_async_remote_copy(
+            src_ref=dec_send.at[g], dst_ref=dec_recv.at[g, r],
+            send_sem=ds_sem.at[g, r], recv_sem=dr_sem.at[g, r],
+            device_id={"sp": partner(me, r)}, device_id_type=MESH,
+        )
+
+    def back_copy(g, r):
+        return pltpu.make_async_remote_copy(
+            src_ref=ret_send.at[g, partner(me, r)], dst_ref=ret_recv.at[owned(g, me)],
+            send_sem=bs_sem.at[g, r], recv_sem=br_sem.at[g, r],
+            device_id={"sp": partner(me, r)}, device_id_type=MESH,
+        )
+
+    def back_from(g, r):
+        return pltpu.make_async_remote_copy(
+            src_ref=ret_send.at[g, me], dst_ref=ret_recv.at[owned(g, partner(me, r))],
+            send_sem=bs_sem.at[g, r], recv_sem=br_sem.at[g, r],
+            device_id={"sp": partner(me, r)}, device_id_type=MESH,
+        )
+
+    others = range(n - 1, 0, -1)
+
     for h in range(heads):
         c = slice(h * HEAD_DIM, (h + 1) * HEAD_DIM)
         key = (1.0 - bound[:, c]) / (1.0 + jnp.exp(logit[:, c].astype(f32)))
@@ -108,41 +142,19 @@
         keys = (key * jnp.exp(mid - cum)).astype(bf16)
         k_scr[:, c] = keys
         st_send[c, :] = (dot(value[:, c], keys, TN) * jnp.exp(mid)).astype(bf16)
-        dec_send[h : h + 1, :] = last
-        if h == (heads - 1) // 2:
+        g = h // per
+        dec_send[g, h % per : h % per + 1, :] = last
+        if h == 0:
             pl.semaphore_wait(barrier, n)
-            for copy in peer + local:
-                copy.start()
-
-    def state_copy(dst, src):
-        return pltpu.make_async_remote_copy(
-            src_ref=st_send.at[rows_of(dst, piece)], dst_ref=st_recv.at[src],
-            send_sem=s_sem.at[dst], recv_sem=r_sem.at[src],
-            device_id={"sp": dst}, device_id_type=MESH,
-        )
-
-    def decay_copy(dst, src):
-        return pltpu.make_async_remote_copy(
-            src_ref=dec_send, dst_ref=dec_recv.at[src],
-            send_sem=ds_sem.at[dst], recv_sem=dr_sem.at[src],
-            device_id={"sp": dst}, device_id_type=MESH,
-        )
-
-    def back_copy(dst, src):
-        return pltpu.make_async_remote_copy(
-            src_ref=ret_send.at[dst], dst_ref=ret_recv.at[rows_of(src, piece)],
-            send_sem=bs_sem.at[dst], recv_sem=br_sem.at[src],
-            device_id={"sp": dst}, device_id_type=MESH,
-        )
-
-    @pl.loop(1, n)
-    def _(r):
-        dst = lax.rem(me + r, n)
-        decay_copy(dst, me).start()
-        state_copy(dst, me).start()
-
-    st_recv[me] = st_send[rows_of(me, piece), :]
-    dec_recv[me] = dec_send[...]
+        if h % per == per - 1:
+            for r in others:
+                decay_copy(g, r).start()
+                state_copy(g, r).start()
+            st_recv[g, 0] = st_send[owned(g, me), :]
+            dec_recv[g, 0] = dec_send[g]
+            if g == 0:
+                for copy in peer + local:
+                    copy.start()
 
     for h in range(heads):
         c = slice(h * HEAD_DIM, (h + 1) * HEAD_DIM)
@@ -180,33 +192,32 @@
     high = combine.astype(bf16)
     both = jnp.concatenate([high, (combine - high.astype(f32)).astype(bf16)], axis=0)
 
-    @pl.loop(1, n)
-    def _(r):
-        src = lax.rem(me + r, n)
-        decay_copy(me, src).wait_recv()
-        state_copy(me, src).wait_recv()
-
-    my_head = me * piece // HEAD_DIM
-
-    def prefix(p, acc):
-        last = dec_recv[p, pl.ds(my_head, 1), :]
-        ret_send[p] = (acc * jnp.exp(0.5 * last)).astype(bf16)
-        return acc * jnp.exp(last) + st_recv[p].astype(f32)
-
-    lax.fori_loop(0, n, prefix, jnp.zeros((piece, HEAD_DIM), f32))
-
-    @pl.loop(1, n)
-    def _(r):
-        back_copy(lax.rem(me + r, n), me).start()
-
-    ret_recv[rows_of(me, piece), :] = ret_send[me]
-
-    @pl.loop(1, n)
-    def _(r):
-        back_copy(me, lax.rem(me + r, n)).wait_recv()
+    for g in range(groups):
+        for r in others:
+            decay_copy(g, r).wait_recv()
+            state_copy(g, r).wait_recv()
+        own_head = me * piece // HEAD_DIM
+
+        def prefix(p, acc):
+            r = 0
+            step = 1
+            while step < n:
+                r = r + step * ((me // step + p // step) % 2)
+                step *= 2
+            last = dec_recv[g, r, pl.ds(own_head, 1), :]
+            ret_send[g, p] = (acc * jnp.exp(0.5 * last)).astype(bf16)
+            return acc * jnp.exp(last) + st_recv[g, r].astype(f32)
+
+        lax.fori_loop(0, n, prefix, jnp.zeros((piece, HEAD_DIM), f32))
+        for r in others:
+            back_copy(g, r).start()
+        ret_recv[owned(g, me), :] = ret_send[g, me]
 
     for h in range(heads):
         c = slice(h * HEAD_DIM, (h + 1) * HEAD_DIM)
+        if h % per == 0:
+            for r in others:
+                back_from(h // per, r).wait_recv()
         out = ho[:, c] + dot(q_scr[:, c], ret_recv[c, :], NT)
         out = out * lax.rsqrt(jnp.mean(out * out, axis=1, keepdims=True) + epsilon)
         g = gate[:, c].astype(f32)
@@ -319,12 +330,11 @@
         back = dot(both, returned[:, cols])
         layer_out[:, cols] = (proj[:, cols] + (back[:count] + back[count:])).astype(bf16)
 
-    @pl.loop(1, n)
-    def _(r):
-        dst = lax.rem(me + r, n)
-        decay_copy(dst, me).wait_send()
-        state_copy(dst, me).wait_send()
-        back_copy(dst, me).wait_send()
+    for g in range(groups):
+        for r in others:
+            decay_copy(g, r).wait_send()
+            state_copy(g, r).wait_send()
+            back_copy(g, r).wait_send()
 
     for r in range(1, n):
         send_copy(r).wait_send()
@@ -347,7 +357,8 @@
         cap = 2 * half * routing.shape[1] // n
         cap = -(-cap // 16) * 16
         slots = n * cap
-        piece = width // n
+        groups = 2 if heads % 2 == 0 and width // n % 32 == 0 else 1
+        piece = width // n // groups
         inner = expert_gate.shape[2]
         top = routing.shape[1]
         return pl.pallas_call(
@@ -371,10 +382,10 @@
                 pltpu.VMEM((length, width), bf16),
                 pltpu.VMEM((length, width), f32),
                 pltpu.VMEM((width, HEAD_DIM), bf16),
-                pltpu.VMEM((n, piece, HEAD_DIM), bf16),
-                pltpu.VMEM((heads, HEAD_DIM), f32),
-                pltpu.VMEM((n, heads, HEAD_DIM), f32),
-                pltpu.VMEM((n, piece, HEAD_DIM), bf16),
+                pltpu.VMEM((groups, n, piece, HEAD_DIM), bf16),
+                pltpu.VMEM((groups, heads // groups, HEAD_DIM), f32),
+                pltpu.VMEM((groups, n, heads // groups, HEAD_DIM), f32),
+                pltpu.VMEM((groups, n, piece, HEAD_DIM), bf16),
                 pltpu.VMEM((width, HEAD_DIM), bf16),
                 pltpu.VMEM((2, half, width), bf16),
                 pltpu.VMEM((half, width), bf16),
@@ -387,7 +398,9 @@
                 pltpu.VMEM((2, slots, inner), bf16),
                 pltpu.VMEM((slots, model), bf16),
                 pltpu.VMEM((slots, model), bf16),
-                dma((10,)), dma, dma((n,)), dma((n,)), dma((n,)), dma((n,)), dma((n,)), dma((n,)),
+                dma((10,)), dma,
+                dma((groups, n)), dma((groups, n)), dma((groups, n)),
+                dma((groups, n)), dma((groups, n)), dma((groups, n)),
                 dma, dma, dma((3,)), dma((3,)), dma((3,)),
                 dma((n,)), dma((n,)), dma((n,)), dma((n,)),
             ],

time: 80.8 us -> 79.5 us (0.984)
  Pallas kernels: 79 us -> 77.7 us
    pallas_call x1, Pallas kernels: 79 us -> 77.7 us  [body(): pl.pallas_call(functools.partial(layer_kernel, n, cap), out_shape=jax.Sha...]
where the time goes in v3:
time: 79.5 us; the launch traced here: 79.3 us
  Pallas kernels  77.7 us (98%)
  local copies, waits for them, and re-layouts  1.67 us (2%)
    pallas_call x1, Pallas kernels, body(): pl.pallas_call(functools.partial(layer_kernel, n, cap), out_shape=jax.Sha...  77.7 us
    unnamed x1, local copies, waits for them, and re-layouts  1.67 us

profile of v3, /device:TPU:0, one launch (start us, length us, event | category | flops | bytes accessed | tf_op | source)
XLA Modules:
  0.0 79.3 jit_solution(12146962437638094104)
XLA Ops:
  0.0 77.7 %shard_map.136 = bf16[64,2048]{1,0:T(8,128)(2,1)} custom-call(bf16[128,1024]{1,0:T(8,128)(2,1)} %query_h.1, bf16[128,1024]{1,0:T(8,128)(2,1)} %logit_h.1, bf16[128,1024]{1,0:T(8,128)(2,1)} %value_h.1, bf16[128,1024]{1,0:T(8,128)(2,1)} %gate_h.1, f32[1,1024]{1,0:T(1,128)} %bitcast.6, f32[1,1024]{1,0:T(1,128)} %bitcast.7, bf16[64,2048]{1,0:T(8,128)(2,1)} %residual_h.1, ...), custom_call_target="tpu_custom_call" | custom-call | tf_op jit(solution)/shard_map/pallas_call | solution.py:364
  77.7 1.7 %copy.16 = bf16[64,2048]{1,0:T(8,128)(2,1)} copy(bf16[64,2048]{1,0:T(8,128)(2,1)} %shard_map.136) | data formatting | bytes 524288
